TPU v7x, 32 devices: a whole 2x2x4 slice. The times are simulated.
32 devices in a mesh: sp: 4 (over z), dp: 8 (over y, x, core).
Axes of the slice: x: 2, y: 2, z: 4, core: 2. Of those that a mesh axis runs over, the one named last changes fastest.
Arguments:
- hidden_states: bfloat16 [8, 512, 2048], P('dp', 'sp'), may hold values from -6 to 6
- queries: bfloat16 [8, 512, 2048], P('dp', 'sp'), may hold values from -12 to 12
- key_shift: bfloat16 [8, 512, 16], P('dp', 'sp'), may hold values from -15 to 0
- key_weight: bfloat16 [2048, 256], P('dp'), may hold values from -0.125 to 0.125
- value_weight: bfloat16 [2048, 256], P('dp'), may hold values from -0.125 to 0.125
Outputs:
- attended: bfloat16 [8, 512, 2048], P('dp', 'sp')
All inputs are finite; a program needn't handle non-finite values.
Results may differ from a plain program's by a relative error of at most 0.0079.
Values may be sent and summed in bfloat16 or wider, within the bound.
A program may use at most 64 MiB of HBM per device.

v0:
```python
import jax
import jax.numpy as jnp
from jax import lax
from jax.sharding import PartitionSpec as P

QUERY_HEAD_COUNT = 16
HEAD_DIM = 128


def attend(queries, key_all, value_all, shift_all):
    length, head_count, head_dim = queries.shape
    block_len = min(512, length)
    block_count = length // block_len
    scaling = head_dim ** (-0.5)
    shift_float = shift_all.astype(jnp.float32)
    offsets = jnp.arange(block_len, dtype=jnp.int32)

    def over_queries(block_index, outputs):
        first_row = block_index * block_len
        query_tile = lax.dynamic_slice_in_dim(queries, first_row, block_len, 0)

        def over_keys(back_step, state_pair):
            running, carried = state_pair
            key_start = (block_index - back_step) * block_len
            key_tile = lax.dynamic_slice_in_dim(key_all, key_start, block_len, 0)
            value_tile = lax.dynamic_slice_in_dim(value_all, key_start, block_len, 0)
            shift_tile = lax.dynamic_slice_in_dim(shift_float, key_start, block_len, 0)
            logits = jnp.einsum(
                "qhd,khd->hqk", query_tile, key_tile, preferred_element_type=jnp.float32
            )
            logits = logits * scaling + shift_tile.T[:, None, :]
            visible = (key_start + offsets)[None, :] < (first_row + offsets)[:, None]
            penalty = jnp.where(visible, jax.nn.softplus(logits), 0.0)
            suffix_sum = lax.cumsum(penalty, axis=2, reverse=True) - penalty + carried[:, :, None]
            weights = jnp.where(
                visible, jnp.exp(jax.nn.log_sigmoid(logits) - suffix_sum), 0.0
            ).astype(jnp.bfloat16)
            running = running + jnp.einsum(
                "hqk,khd->hqd", weights, value_tile, preferred_element_type=jnp.float32
            )
            return (running, carried + jnp.sum(penalty, axis=2))

        initial = (
            jnp.zeros((head_count, block_len, head_dim), jnp.float32),
            jnp.zeros((head_count, block_len), jnp.float32),
        )
        running, carried = lax.fori_loop(0, block_index + 1, over_keys, initial)
        finished = jnp.transpose(running, (1, 0, 2)).astype(jnp.bfloat16)
        return lax.dynamic_update_slice_in_dim(outputs, finished, first_row, 0)

    return lax.fori_loop(0, block_count, over_queries, jnp.zeros(queries.shape, jnp.bfloat16))


def per_device(hidden_states, queries, key_shift, key_weight, value_weight):
    seq_local, tok_local, model_dim = hidden_states.shape
    token_rows = hidden_states.reshape(seq_local * tok_local, model_dim)
    key_sum = jnp.dot(
        token_rows,
        lax.all_gather(key_weight, "dp", axis=0, tiled=True),
        preferred_element_type=jnp.float32,
    )
    value_sum = jnp.dot(
        token_rows,
        lax.all_gather(value_weight, "dp", axis=0, tiled=True),
        preferred_element_type=jnp.float32,
    )
    shared_heads = key_weight.shape[1] // HEAD_DIM
    key_local = key_sum.astype(jnp.bfloat16).reshape(seq_local, tok_local, shared_heads, HEAD_DIM)
    value_local = value_sum.astype(jnp.bfloat16).reshape(
        seq_local, tok_local, shared_heads, HEAD_DIM
    )
    query_local = queries.reshape(seq_local, tok_local, QUERY_HEAD_COUNT, HEAD_DIM)
    group_size = QUERY_HEAD_COUNT // shared_heads
    key_wide = jnp.repeat(key_local, group_size, axis=2)
    value_wide = jnp.repeat(value_local, group_size, axis=2)
    query_heads, key_heads, value_heads, shift_heads = (
        lax.all_to_all(query_local, "sp", split_axis=2, concat_axis=1, tiled=True),
        lax.all_to_all(key_wide, "sp", split_axis=2, concat_axis=1, tiled=True),
        lax.all_to_all(value_wide, "sp", split_axis=2, concat_axis=1, tiled=True),
        lax.all_to_all(key_shift, "sp", split_axis=2, concat_axis=1, tiled=True),
    )
    outputs = jax.vmap(attend)(query_heads, key_heads, value_heads, shift_heads)
    returned = lax.all_to_all(outputs, "sp", split_axis=1, concat_axis=2, tiled=True)
    return returned.reshape(seq_local, tok_local, QUERY_HEAD_COUNT * HEAD_DIM)


def solution(mesh):
    placed = (
        P("dp", "sp", None),
        P("dp", "sp", None),
        P("dp", "sp", None),
        P("dp", None),
        P("dp", None),
    )
    return jax.shard_map(
        per_device, mesh=mesh, in_specs=placed, out_specs=P("dp", "sp", None), check_vma=False
    )
```

profile of v0, /device:TPU:0, one launch (start us, length us, event | category | flops | bytes accessed | tf_op | source)
XLA Modules:
  0.0 132.7 jit_solution(17721567945287426333)
XLA Ops:
  6.5 0.7 all-gather.3.cloned.1.call-update
  7.3 0.0 all-gather.5.cloned.1.call-start
  7.3 0.7 all-gather.5.cloned.1.call-update
  8.0 0.7 copy.54
  8.7 0.5 broadcast.134
  9.2 0.7 reduce.9
  9.9 0.6 reshape.251
  10.5 6.3 %all-to-all-start.2 = ((bf16[4,2,256]{2,1,0:T(2,128)(2,1)}), bf16[4,2,256]{2,1,0:T(2,128)(2,1)S(1)}, u32[]{:S(2)}, u32[]{:S(2)}) async-start(bf16[4,2,256]{2,1,0:T(2,128)(2,1)} %reshape.251), calls=%async_computation.2 | async-start | bytes 8192 | tf_op jit(solution)/shard_map/all_to_all | solution.py:80
  16.8 2.0 %copy.32 = bf16[1,128,2048]{1,2,0:T(8,128)(2,1)} copy(bf16[1,128,2048]{2,1,0:T(8,128)(2,1)} %param.8) | data formatting | bytes 1048576 | tf_op args[1]
  18.9 3.4 %all-to-all-done.2 = bf16[4,2,256]{2,1,0:T(2,128)(2,1)S(1)} async-done(((bf16[4,2,256]{2,1,0:T(2,128)(2,1)}), bf16[4,2,256]{2,1,0:T(2,128)(2,1)S(1)}, u32[]{:S(2)}, u32[]{:S(2)}) %all-to-all-start.2) | async-done | bytes 4128 | tf_op jit(solution)/shard_map/all_to_all | solution.py:80
  22.3 3.5 %all-to-all-start = ((bf16[1,128,16,128]{1,3,0,2:T(8,128)(2,1)}), bf16[1,128,16,128]{1,3,0,2:T(8,128)(2,1)S(1)}, u32[]{:S(2)}, u32[]{:S(2)}) async-start(bf16[1,128,16,128]{1,3,0,2:T(8,128)(2,1)} %bitcast.6), calls=%async_computation | async-start | bytes 1048576 | tf_op jit(solution)/shard_map/all_to_all | solution.py:77
  25.8 9.6 %all-gather.3.cloned.1.call-done = bf16[2048,256]{1,0:T(8,128)(2,1)} async-done(((bf16[256,256]{1,0:T(8,128)(2,1)}), bf16[2048,256]{1,0:T(8,128)(2,1)}) %all-gather.3.cloned.1.call-update) | async-done | bytes 1048592 | tf_op jit(solution)/shard_map/all_gather | solution.py:59
  35.4 1.5 %fusion.14 = bf16[16,2,8,128]{3,2,1,0:T(8,128)(2,1)S(1)} fusion(bf16[2048,256]{1,0:T(8,128)(2,1)} %all-gather.3.cloned.1.call-done, bf16[1,128,2048]{2,1,0:T(8,128)(2,1)S(1)} %copy-done), kind=kOutput, calls=%fused_computation.24 | convolution fusion | flops 134250496 | bytes 1638400 | tf_op jit(solution)/shard_map/dot_general | solution.py:57
  36.9 2.3 %all-to-all-done = bf16[1,128,16,128]{1,3,0,2:T(8,128)(2,1)S(1)} async-done(((bf16[1,128,16,128]{1,3,0,2:T(8,128)(2,1)}), bf16[1,128,16,128]{1,3,0,2:T(8,128)(2,1)S(1)}, u32[]{:S(2)}, u32[]{:S(2)}) %all-to-all-start) | async-done | bytes 524320 | tf_op jit(solution)/shard_map/all_to_all | solution.py:77
  39.2 0.9 broadcast_in_dim.36
  40.1 3.5 %all-to-all-start.1 = ((bf16[1,128,16,128]{3,1,0,2:T(8,128)(2,1)}), bf16[1,128,16,128]{3,1,0,2:T(8,128)(2,1)S(1)}, u32[]{:S(2)}, u32[]{:S(2)}) async-start(bf16[1,128,16,128]{3,1,0,2:T(8,128)(2,1)} %bitcast.1), calls=%async_computation.1 | async-start | bytes 1048576 | tf_op jit(solution)/shard_map/all_to_all | solution.py:78
  43.6 0.1 iota_compare_fusion
  43.7 0.3 copy.34
  44.0 16.6 %all-gather.5.cloned.1.call-done = bf16[2048,256]{1,0:T(8,128)(2,1)} async-done(((bf16[256,256]{1,0:T(8,128)(2,1)}), bf16[2048,256]{1,0:T(8,128)(2,1)}) %all-gather.5.cloned.1.call-update) | async-done | bytes 1048592 | tf_op jit(solution)/shard_map/all_gather | solution.py:64
  60.6 1.5 %fusion.15 = bf16[16,2,8,128]{3,2,1,0:T(8,128)(2,1)S(1)} fusion(bf16[2048,256]{1,0:T(8,128)(2,1)} %all-gather.5.cloned.1.call-done, bf16[1,128,2048]{2,1,0:T(8,128)(2,1)S(1)} %copy-done), kind=kOutput, calls=%fused_computation.25 | convolution fusion | flops 134250496 | bytes 1638400 | tf_op jit(solution)/shard_map/dot_general | solution.py:62
  62.2 0.9 broadcast_in_dim.38
  63.1 4.6 %all-to-all-start.3 = ((bf16[1,128,16,128]{3,1,0,2:T(8,128)(2,1)}), bf16[1,128,16,128]{3,1,0,2:T(8,128)(2,1)S(1)}, u32[]{:S(2)}, u32[]{:S(2)}) async-start(bf16[1,128,16,128]{3,1,0,2:T(8,128)(2,1)} %bitcast.21), calls=%async_computation.3 | async-start | bytes 1048576 | tf_op jit(solution)/shard_map/all_to_all | solution.py:79
  67.7 4.4 %fusion.5 = (f32[4,512,512]{1,2,0:T(8,128)S(1)}, f32[4,512,512]{2,1,0:T(8,128)}) fusion(f32[4,512]{1,0:T(4,128)S(1)} %bitcast.103, pred[512,512]{0,1:T(8,128)(4,1)S(1)} %iota_compare_fusion, bf16[512,4,128]{2,0,1:T(8,128)(2,1)S(1)} %bitcast.100, bf16[512,4,128]{2,0,1:T(8,128)(2,1)S(1)} %bitcast.99), kind=kOutput, calls=%fused_computation.7 | convolution fusion | flops 277872640 | bytes 9707520 | tf_op jit(solution)/shard_map/vmap()/while/body/eval_jaxpr/while/body/qhd,khd->hqk/dot_general | solution.py:28
  72.2 19.6 %fusion.11 = f32[1,4,512,4,128]{2,3,4,1,0:T(4,128)S(1)} fusion(f32[1,4,512,4,128]{2,4,3,1,0:T(8,128)S(1)} %bitcast.93), kind=kOutput, calls=%fused_computation.17 | output fusion | flops 133169152 | bytes 8388608 | tf_op jit(solution)/shard_map/reduce-window.8
  91.8 3.3 %copy.38 = f32[1,4,512,4,128]{2,4,3,1,0:T(8,128)} copy(f32[1,4,512,4,128]{2,3,4,1,0:T(4,128)S(1)} %fusion.11) | data formatting | bytes 8388608 | tf_op jit(solution)/shard_map/reduce-window.8
  95.0 0.1 reduce-window.19
  95.2 8.8 %fusion.4 = bf16[4,512,512]{1,2,0:T(8,128)(2,1)S(1)} fusion(f32[4,512,512]{1,2,0:T(8,128)} %bitcast.92, f32[4,512,512]{2,1,0:T(8,128)} %get-tuple-element.133, f32[4,512]{1,0:T(4,128)S(1)} %bitcast.104, f32[4,512,4]{1,2,0:T(4,128)S(1)} %slice_bitcast_fusion, pred[512,512]{0,1:T(8,128)(4,1)S(1)} %iota_compare_fusion), kind=kLoop, calls=%fused_computation.6 | loop fusion | flops 23068672 | bytes 10788864 | tf_op jit(solution)/shard_map/vmap()/while/body/eval_jaxpr/while/body/convert_element_type | solution.py:37
  104.0 0.9 fusion.13
  104.9 0.4 copy.42
  105.3 19.2 %all_to_all.78 = bf16[1,512,4,128]{3,2,0,1:T(4,128)(2,1)S(1)} all-to-all(bf16[1,512,4,128]{3,2,0,1:T(4,128)(2,1)S(1)} %copy.42), channel_id=1, replica_groups=mesh['sp'=4,'dp'=8] {'sp'}, dimensions={1} | all-to-all | bytes 1048576 | tf_op jit(solution)/shard_map/all_to_all | solution.py:83
  124.5 0.2 copy.43
  124.7 1.2 reshape.241
  (14 shorter events, 0.2 us)
Async XLA Ops:
  6.5 28.8 %copy-start = (bf16[1,128,2048]{2,1,0:T(8,128)(2,1)S(1)}, bf16[1,128,2048]{2,1,0:T(8,128)(2,1)}, u32[]{:S(2)}) copy-start(bf16[1,128,2048]{2,1,0:T(8,128)(2,1)} %param.7) | copy-start | bytes 1572868
  6.5 28.8 %all-gather.3.cloned.1.call-start = ((), (), s32[]{:S(2)}) async-start(), calls=%async_computation.5 | async-start | bytes 1179648 | tf_op jit(solution)/shard_map/all_gather | solution.py:59
  7.3 53.4 %all-gather.5.cloned.1.call-start = ((), (), s32[]{:S(2)}) async-start(), calls=%async_computation.6 | async-start | bytes 1179648 | tf_op jit(solution)/shard_map/all_gather | solution.py:64
  10.5 11.8 %all-to-all-start.2 = ((bf16[4,2,256]{2,1,0:T(2,128)(2,1)}), bf16[4,2,256]{2,1,0:T(2,128)(2,1)S(1)}, u32[]{:S(2)}, u32[]{:S(2)}) async-start(bf16[4,2,256]{2,1,0:T(2,128)(2,1)} %reshape.251), calls=%async_computation.2 | async-start | bytes 8192 | tf_op jit(solution)/shard_map/all_to_all | solution.py:80
  22.3 16.9 %all-to-all-start = ((bf16[1,128,16,128]{1,3,0,2:T(8,128)(2,1)}), bf16[1,128,16,128]{1,3,0,2:T(8,128)(2,1)S(1)}, u32[]{:S(2)}, u32[]{:S(2)}) async-start(bf16[1,128,16,128]{1,3,0,2:T(8,128)(2,1)} %bitcast.6), calls=%async_computation | async-start | bytes 1048576 | tf_op jit(solution)/shard_map/all_to_all | solution.py:77
  40.1 22.1 %all-to-all-start.1 = ((bf16[1,128,16,128]{3,1,0,2:T(8,128)(2,1)}), bf16[1,128,16,128]{3,1,0,2:T(8,128)(2,1)S(1)}, u32[]{:S(2)}, u32[]{:S(2)}) async-start(bf16[1,128,16,128]{3,1,0,2:T(8,128)(2,1)} %bitcast.1), calls=%async_computation.1 | async-start | bytes 1048576 | tf_op jit(solution)/shard_map/all_to_all | solution.py:78
  63.1 32.0 %all-to-all-start.3 = ((bf16[1,128,16,128]{3,1,0,2:T(8,128)(2,1)}), bf16[1,128,16,128]{3,1,0,2:T(8,128)(2,1)S(1)}, u32[]{:S(2)}, u32[]{:S(2)}) async-start(bf16[1,128,16,128]{3,1,0,2:T(8,128)(2,1)} %bitcast.21), calls=%async_computation.3 | async-start | bytes 1048576 | tf_op jit(solution)/shard_map/all_to_all | solution.py:79
Sparse Core Ops, SparseCore 0:
  9.2 26.0 all-gather.2
  37.2 23.3 all-gather.4
where the time goes:
time: 133 us
  waiting for transfers between devices  33.3 us (25%)
  other arithmetic  29.2 us (22%)
  blocking collectives  19.2 us (14%)
  starting transfers between devices  17.9 us (13%)
  between operations  13.6 us (10%)
  local copies, waits for them, and re-layouts  11.1 us (8%)
  matrix products  8.43 us (6%)
    another operation x2, other arithmetic  19.6 us
    all_to_all x1, blocking collectives, per_device(): lax.all_to_all(outputs, 'sp', split_axis=1, concat_axis=2, tiled=True)  19.2 us
    all_gather x1, waiting for transfers between devices, per_device(): lax.all_gather(value_weight, 'dp', axis=0, tiled=True)  16.6 us
    all_gather x1, waiting for transfers between devices, per_device(): lax.all_gather(key_weight, 'dp', axis=0, tiled=True)  9.59 us
    convert_element_type x1, other arithmetic, over_keys(): weights = jnp.where(visible, jnp.exp(jax.nn.log_sigmoid(logits) - suffix_...  8.78 us
    all_to_all x1, starting transfers between devices, per_device(): lax.all_to_all(key_shift, 'sp', split_axis=2, concat_axis=1, tiled=True)  6.35 us
    all_to_all x1, starting transfers between devices, per_device(): lax.all_to_all(value_wide, 'sp', split_axis=2, concat_axis=1, tiled=True)  4.6 us
    dot_general x1, matrix products, over_keys(): jnp.einsum('qhd,khd->hqk', query_tile, key_tile, preferred_element_type=j...  4.44 us
  transfers between devices with their start and end apart: 6, of which 4 were waited for; matrix products, arithmetic and copies ran while one was open for 27% of the time, Pallas kernels for 0%

commit v1 on v0

--- a/solution.py
+++ b/solution.py
@@ -5,6 +5,12 @@
 
 QUERY_HEAD_COUNT = 16
 HEAD_DIM = 128
+
+
+def exchange_blocks(value, axis, split, join):
+    parts = jnp.split(value, lax.axis_size(axis), axis=split)
+    got = lax.all_to_all(jnp.stack(parts), axis, 0, 0)
+    return jnp.concatenate(got, axis=join)
 
 
 def attend(queries, key_all, value_all, shift_all):
@@ -77,7 +83,7 @@
         lax.all_to_all(query_local, "sp", split_axis=2, concat_axis=1, tiled=True),
         lax.all_to_all(key_wide, "sp", split_axis=2, concat_axis=1, tiled=True),
         lax.all_to_all(value_wide, "sp", split_axis=2, concat_axis=1, tiled=True),
-        lax.all_to_all(key_shift, "sp", split_axis=2, concat_axis=1, tiled=True),
+        exchange_blocks(key_shift, "sp", 2, 1),
     )
     outputs = jax.vmap(attend)(query_heads, key_heads, value_heads, shift_heads)
     returned = lax.all_to_all(outputs, "sp", split_axis=1, concat_axis=2, tiled=True)

time: 133 us -> 133 us (level)
    unnamed x7 -> x3, local copies, waits for them, and re-layouts: 3.87 us -> 2.04 us
    another operation x3 -> x4, local copies, waits for them, and re-layouts: 3.28 us -> 4.03 us
    another operation x2 -> x3, other arithmetic: 19.6 us -> 20.2 us
where the time goes in v1:
time: 133 us
  waiting for transfers between devices  34.4 us (26%)
  other arithmetic  29.1 us (22%)
  blocking collectives  19.2 us (14%)
  starting transfers between devices  17.9 us (13%)
  between operations  13.5 us (10%)
  local copies, waits for them, and re-layouts  10.1 us (8%)
  matrix products  8.45 us (6%)
    another operation x2, other arithmetic  19.6 us
    all_to_all x1, blocking collectives, per_device(): lax.all_to_all(outputs, 'sp', split_axis=1, concat_axis=2, tiled=True)  19.2 us
    all_gather x1, waiting for transfers between devices, per_device(): lax.all_gather(value_weight, 'dp', axis=0, tiled=True)  17.7 us
    all_gather x1, waiting for transfers between devices, per_device(): lax.all_gather(key_weight, 'dp', axis=0, tiled=True)  10.6 us
    convert_element_type x1, other arithmetic, over_keys(): weights = jnp.where(visible, jnp.exp(jax.nn.log_sigmoid(logits) - suffix_...  8.78 us
    all_to_all x1, starting transfers between devices, exchange_blocks(): got = lax.all_to_all(jnp.stack(parts), axis, 0, 0)  6.35 us
    all_to_all x1, starting transfers between devices, per_device(): lax.all_to_all(value_wide, 'sp', split_axis=2, concat_axis=1, tiled=True)  4.6 us
    dot_general x1, matrix products, over_keys(): jnp.einsum('qhd,khd->hqk', query_tile, key_tile, preferred_element_type=j...  4.46 us
  transfers between devices with their start and end apart: 6, of which 4 were waited for; matrix products, arithmetic and copies ran while one was open for 27% of the time, Pallas kernels for 0%

profile of v1, /device:TPU:0, one launch (start us, length us, event | category | flops | bytes accessed | tf_op | source)
XLA Modules:
  0.0 132.7 jit_solution(2154741263389265936)
XLA Ops:
  6.5 0.7 all-gather.3.cloned.1.call-update
  7.3 0.0 all-gather.5.cloned.1.call-start
  7.3 0.7 all-gather.5.cloned.1.call-update
  8.0 0.8 slice_bitcast_fusion.5
  8.8 0.6 pad_maximum_fusion
  9.4 6.3 %all-to-all-start.2 = ((bf16[4,1,128,4]{2,3,1,0:T(4,128)(2,1)}), bf16[4,1,128,4]{2,3,1,0:T(4,128)(2,1)S(1)}, u32[]{:S(2)}, u32[]{:S(2)}) async-start(bf16[4,1,128,4]{2,3,1,0:T(4,128)(2,1)} %pad_maximum_fusion), calls=%async_computation.2 | async-start | bytes 8192 | tf_op jit(solution)/shard_map/all_to_all | solution.py:12
  15.7 2.0 %copy.32 = bf16[1,128,2048]{1,2,0:T(8,128)(2,1)} copy(bf16[1,128,2048]{2,1,0:T(8,128)(2,1)} %param.8) | data formatting | bytes 1048576 | tf_op args[1]
  17.8 3.5 %all-to-all-done.2 = bf16[4,1,128,4]{2,3,1,0:T(4,128)(2,1)S(1)} async-done(((bf16[4,1,128,4]{2,3,1,0:T(4,128)(2,1)}), bf16[4,1,128,4]{2,3,1,0:T(4,128)(2,1)S(1)}, u32[]{:S(2)}, u32[]{:S(2)}) %all-to-all-start.2) | async-done | bytes 4128 | tf_op jit(solution)/shard_map/all_to_all | solution.py:12
  21.3 3.5 %all-to-all-start = ((bf16[1,128,16,128]{1,3,0,2:T(8,128)(2,1)}), bf16[1,128,16,128]{1,3,0,2:T(8,128)(2,1)S(1)}, u32[]{:S(2)}, u32[]{:S(2)}) async-start(bf16[1,128,16,128]{1,3,0,2:T(8,128)(2,1)} %bitcast.6), calls=%async_computation | async-start | bytes 1048576 | tf_op jit(solution)/shard_map/all_to_all | solution.py:83
  24.8 10.6 %all-gather.3.cloned.1.call-done = bf16[2048,256]{1,0:T(8,128)(2,1)} async-done(((bf16[256,256]{1,0:T(8,128)(2,1)}), bf16[2048,256]{1,0:T(8,128)(2,1)}) %all-gather.3.cloned.1.call-update) | async-done | bytes 1048592 | tf_op jit(solution)/shard_map/all_gather | solution.py:65
  35.4 1.5 %fusion.14 = bf16[16,2,8,128]{3,2,1,0:T(8,128)(2,1)S(1)} fusion(bf16[2048,256]{1,0:T(8,128)(2,1)} %all-gather.3.cloned.1.call-done, bf16[1,128,2048]{2,1,0:T(8,128)(2,1)S(1)} %copy-done), kind=kOutput, calls=%fused_computation.24 | convolution fusion | flops 134250496 | bytes 1638400 | tf_op jit(solution)/shard_map/dot_general | solution.py:63
  36.9 1.2 all-to-all-done
  38.1 0.9 broadcast_in_dim.36
  39.0 3.5 %all-to-all-start.1 = ((bf16[1,128,16,128]{3,1,0,2:T(8,128)(2,1)}), bf16[1,128,16,128]{3,1,0,2:T(8,128)(2,1)S(1)}, u32[]{:S(2)}, u32[]{:S(2)}) async-start(bf16[1,128,16,128]{3,1,0,2:T(8,128)(2,1)} %bitcast.1), calls=%async_computation.1 | async-start | bytes 1048576 | tf_op jit(solution)/shard_map/all_to_all | solution.py:84
  42.5 0.1 iota_compare_fusion
  42.6 0.3 copy.34
  42.9 17.7 %all-gather.5.cloned.1.call-done = bf16[2048,256]{1,0:T(8,128)(2,1)} async-done(((bf16[256,256]{1,0:T(8,128)(2,1)}), bf16[2048,256]{1,0:T(8,128)(2,1)}) %all-gather.5.cloned.1.call-update) | async-done | bytes 1048592 | tf_op jit(solution)/shard_map/all_gather | solution.py:70
  60.6 1.5 %fusion.15 = bf16[16,2,8,128]{3,2,1,0:T(8,128)(2,1)S(1)} fusion(bf16[2048,256]{1,0:T(8,128)(2,1)} %all-gather.5.cloned.1.call-done, bf16[1,128,2048]{2,1,0:T(8,128)(2,1)S(1)} %copy-done), kind=kOutput, calls=%fused_computation.25 | convolution fusion | flops 134250496 | bytes 1638400 | tf_op jit(solution)/shard_map/dot_general | solution.py:68
  62.2 0.0 all-to-all-done.1
  62.2 0.9 broadcast_in_dim.38
  63.1 4.6 %all-to-all-start.3 = ((bf16[1,128,16,128]{3,1,0,2:T(8,128)(2,1)}), bf16[1,128,16,128]{3,1,0,2:T(8,128)(2,1)S(1)}, u32[]{:S(2)}, u32[]{:S(2)}) async-start(bf16[1,128,16,128]{3,1,0,2:T(8,128)(2,1)} %bitcast.23), calls=%async_computation.3 | async-start | bytes 1048576 | tf_op jit(solution)/shard_map/all_to_all | solution.py:85
  67.7 4.5 %fusion.5 = (f32[4,512,512]{1,2,0:T(8,128)S(1)}, f32[4,512,512]{2,1,0:T(8,128)}) fusion(f32[4,512]{1,0:T(4,128)S(1)} %convert_bitcast_fusion, pred[512,512]{0,1:T(8,128)(4,1)S(1)} %iota_compare_fusion, bf16[512,4,128]{2,0,1:T(8,128)(2,1)S(1)} %bitcast.101, bf16[512,4,128]{2,0,1:T(8,128)(2,1)S(1)} %bitcast.100), kind=kOutput, calls=%fused_computation.7 | convolution fusion | flops 277872640 | bytes 9707520 | tf_op jit(solution)/shard_map/vmap()/while/body/eval_jaxpr/while/body/qhd,khd->hqk/dot_general | solution.py:34
  72.2 19.6 %fusion.11 = f32[1,4,512,4,128]{2,3,4,1,0:T(4,128)S(1)} fusion(f32[1,4,512,4,128]{2,4,3,1,0:T(8,128)S(1)} %bitcast.94), kind=kOutput, calls=%fused_computation.17 | output fusion | flops 133169152 | bytes 8388608 | tf_op jit(solution)/shard_map/reduce-window.8
  91.8 3.3 %copy.37 = f32[1,4,512,4,128]{2,4,3,1,0:T(8,128)} copy(f32[1,4,512,4,128]{2,3,4,1,0:T(4,128)S(1)} %fusion.11) | data formatting | bytes 8388608 | tf_op jit(solution)/shard_map/reduce-window.8
  95.0 0.1 reduce-window.19
  95.1 0.0 all-to-all-done.3
  95.2 8.8 %fusion.4 = bf16[4,512,512]{1,2,0:T(8,128)(2,1)S(1)} fusion(f32[4,512,512]{1,2,0:T(8,128)} %bitcast.93, f32[4,512,512]{2,1,0:T(8,128)} %get-tuple-element.137, f32[4,512]{1,0:T(4,128)S(1)} %convert_bitcast_fusion, f32[4,512,4]{1,2,0:T(4,128)S(1)} %slice_bitcast_fusion, pred[512,512]{0,1:T(8,128)(4,1)S(1)} %iota_compare_fusion), kind=kLoop, calls=%fused_computation.6 | loop fusion | flops 23068672 | bytes 10788864 | tf_op jit(solution)/shard_map/vmap()/while/body/eval_jaxpr/while/body/convert_element_type | solution.py:43
  104.0 0.9 fusion.13
  104.9 0.4 copy.41
  105.3 19.2 %all_to_all.74 = bf16[1,512,4,128]{3,2,0,1:T(4,128)(2,1)S(1)} all-to-all(bf16[1,512,4,128]{3,2,0,1:T(4,128)(2,1)S(1)} %copy.41), channel_id=1, replica_groups=mesh['sp'=4,'dp'=8] {'sp'}, dimensions={1} | all-to-all | bytes 1048576 | tf_op jit(solution)/shard_map/all_to_all | solution.py:89
  124.5 0.2 copy.42
  124.7 1.2 reshape.240
  (11 shorter events, 0.2 us)
Async XLA Ops:
  6.5 28.8 %copy-start = (bf16[1,128,2048]{2,1,0:T(8,128)(2,1)S(1)}, bf16[1,128,2048]{2,1,0:T(8,128)(2,1)}, u32[]{:S(2)}) copy-start(bf16[1,128,2048]{2,1,0:T(8,128)(2,1)} %param.7) | copy-start | bytes 1572868
  6.5 28.8 %all-gather.3.cloned.1.call-start = ((), (), s32[]{:S(2)}) async-start(), calls=%async_computation.5 | async-start | bytes 1179648 | tf_op jit(solution)/shard_map/all_gather | solution.py:65
  7.3 53.4 %all-gather.5.cloned.1.call-start = ((), (), s32[]{:S(2)}) async-start(), calls=%async_computation.6 | async-start | bytes 1179648 | tf_op jit(solution)/shard_map/all_gather | solution.py:70
  9.4 11.9 %all-to-all-start.2 = ((bf16[4,1,128,4]{2,3,1,0:T(4,128)(2,1)}), bf16[4,1,128,4]{2,3,1,0:T(4,128)(2,1)S(1)}, u32[]{:S(2)}, u32[]{:S(2)}) async-start(bf16[4,1,128,4]{2,3,1,0:T(4,128)(2,1)} %pad_maximum_fusion), calls=%async_computation.2 | async-start | bytes 8192 | tf_op jit(solution)/shard_map/all_to_all | solution.py:12
  21.3 16.8 %all-to-all-start = ((bf16[1,128,16,128]{1,3,0,2:T(8,128)(2,1)}), bf16[1,128,16,128]{1,3,0,2:T(8,128)(2,1)S(1)}, u32[]{:S(2)}, u32[]{:S(2)}) async-start(bf16[1,128,16,128]{1,3,0,2:T(8,128)(2,1)} %bitcast.6), calls=%async_computation | async-start | bytes 1048576 | tf_op jit(solution)/shard_map/all_to_all | solution.py:83
  39.0 23.2 %all-to-all-start.1 = ((bf16[1,128,16,128]{3,1,0,2:T(8,128)(2,1)}), bf16[1,128,16,128]{3,1,0,2:T(8,128)(2,1)S(1)}, u32[]{:S(2)}, u32[]{:S(2)}) async-start(bf16[1,128,16,128]{3,1,0,2:T(8,128)(2,1)} %bitcast.1), calls=%async_computation.1 | async-start | bytes 1048576 | tf_op jit(solution)/shard_map/all_to_all | solution.py:84
  63.1 32.0 %all-to-all-start.3 = ((bf16[1,128,16,128]{3,1,0,2:T(8,128)(2,1)}), bf16[1,128,16,128]{3,1,0,2:T(8,128)(2,1)S(1)}, u32[]{:S(2)}, u32[]{:S(2)}) async-start(bf16[1,128,16,128]{3,1,0,2:T(8,128)(2,1)} %bitcast.23), calls=%async_computation.3 | async-start | bytes 1048576 | tf_op jit(solution)/shard_map/all_to_all | solution.py:85
Sparse Core Ops, SparseCore 0:
  9.2 26.0 all-gather.2
  37.2 23.3 all-gather.4
